TPU v7x, 128 devices: a whole 4x4x4 slice. The times are simulated.
128 devices in a mesh: sp: 64 (over z, y, x), tp: 2 (over core).
Axes of the slice: x: 4, y: 4, z: 4, core: 2. Of those that a mesh axis runs over, the one named last changes fastest.
Arguments:
- residual: bfloat16 [16384, 2048], P(('sp', 'tp')), may hold values from -6 to 6
- queries: bfloat16 [16384, 1152], P('sp', 'tp'), may hold values from -800 to 800
- latent: bfloat16 [16384, 256], P('sp'), may hold values from -6 to 6
- rope_key: bfloat16 [16384, 32], P('sp'), may hold values from -6 to 6
- doc_ids: int32 [16384], P('sp'), may hold values from 0 to 5, never falling along the last dimension, each value on 1 to 8192 neighbouring positions
- latent_to_key: bfloat16 [256, 768], P(None, 'tp'), may hold values from -0.375 to 0.375
- latent_to_value: bfloat16 [256, 768], P(None, 'tp'), may hold values from -0.375 to 0.375
- out_proj: bfloat16 [768, 2048], replicated, may hold values from -0.21875 to 0.21875
- mix_gain: float32 [2048], replicated, may hold values from 0.1 to 1.9
- moe_gain: float32 [2048], replicated, may hold values from 0.1 to 1.9
- expert_ids: int32 [16384, 2], P(('sp', 'tp')), may hold values from 0 to 63, as said below
- route_weight: float32 [16384, 2], P(('sp', 'tp')), may hold values from 0.1 to 1
- gate_weight: bfloat16 [64, 2048, 1024], P('sp', None, 'tp'), may hold values from -0.125 to 0.125
- up_weight: bfloat16 [64, 2048, 1024], P('sp', None, 'tp'), may hold values from -0.125 to 0.125
- down_weight: bfloat16 [64, 1024, 2048], P('sp', 'tp'), may hold values from -0.1875 to 0.1875
Outputs:
- output: bfloat16 [16384, 2048], P(('sp', 'tp'))
Inputs may be any that keep to these rules, and one draw needn't show every extreme that they name: `expert_ids`: each row names 2 different experts of one group of 16 consecutive numbers; in each aligned block of 128 rows (the rows of one device) no expert is named more than 8 times, and some expert exactly 8 times.
All inputs are finite; a program needn't handle non-finite values.
Results may differ from a plain program's by a relative error of at most 0.013.
Values may be sent and summed in bfloat16 or wider, within the bound.
A program may use at most 64 MiB of HBM per device.

v0:
```python
import math
import jax
import jax.numpy as jnp
from jax import lax
from jax.sharding import PartitionSpec as P

D = 2048
UNROTATED_DIM = 64
ROPE = 32
VALUE_ENTRIES = 64
GROUPS = 4
rope_base = 10000.0
epsilon = 1e-06


def in_order(pieces, dim):
    pieces = jnp.moveaxis(pieces, 0, dim)
    lengths = pieces.shape
    return pieces.reshape(*lengths[:dim], lengths[dim] * lengths[dim + 1], *lengths[dim + 2 :])


def sent_to_all(x, axis):
    size = lax.axis_size(axis)
    return lax.all_to_all(jnp.broadcast_to(x[None], (size, *x.shape)), axis, 0, 0, tiled=True)


def collect(x, axis, dim):
    return in_order(sent_to_all(x, axis), dim)


def cut_along(x, dim, size):
    before, after = (x.shape[:dim], x.shape[dim + 1 :])
    return jnp.moveaxis(x.reshape(*before, size, -1, *after), dim, 0)


def sum_at_owner(x, axis, dim):
    pieces = cut_along(x, dim, lax.axis_size(axis))
    arrived = lax.all_to_all(pieces, axis, split_axis=0, concat_axis=0, tiled=True)
    return arrived.astype(jnp.float32).sum(axis=0)


def rotate(source, positions):
    half_width = source.shape[-1] // 2
    frequency = rope_base ** (-jnp.arange(half_width, dtype=jnp.float32) / half_width)
    angles = positions.astype(jnp.float32)[:, None] * frequency[None, :]
    if source.ndim == 3:
        angles = angles[:, None, :]
    cosine = jnp.cos(angles)
    sine_part = jnp.sin(angles)
    upper_half = source[..., :half_width].astype(jnp.float32)
    lower_half = source[..., half_width:].astype(jnp.float32)
    turned = jnp.concatenate(
        [
            upper_half * cosine - lower_half * sine_part,
            lower_half * cosine + upper_half * sine_part,
        ],
        axis=-1,
    )
    return turned.astype(jnp.bfloat16)


def rms_scale(source, gain):
    return source * lax.rsqrt(jnp.mean(source * source, axis=-1, keepdims=True) + epsilon) * gain


def attend_keys(
    running,
    query_nope,
    query_rot,
    query_pos,
    query_docs,
    key_nope,
    key_rot,
    value_rows,
    key_pos,
    key_docs,
):
    row_max, row_total, weighted = running
    score_scale = (UNROTATED_DIM + ROPE) ** (-0.5)
    scores = (
        jnp.einsum("qhd,khd->qhk", query_nope, key_nope, preferred_element_type=jnp.float32)
        + jnp.einsum("qhr,kr->qhk", query_rot, key_rot, preferred_element_type=jnp.float32)
    ) * score_scale
    allowed = (
        (key_pos[None, :] <= query_pos[:, None]) & (key_docs[None, :] == query_docs[:, None])
    )[:, None, :]
    new_max = jnp.maximum(row_max, jnp.max(jnp.where(allowed, scores, -1e30), axis=-1))
    weights = jnp.where(allowed, jnp.exp(scores - new_max[..., None]), 0.0)
    factor = jnp.exp(row_max - new_max)
    row_total = row_total * factor + jnp.sum(weights, axis=-1)
    weighted = weighted * factor[..., None] + jnp.einsum(
        "qhk,khd->qhd", weights.astype(jnp.bfloat16), value_rows, preferred_element_type=jnp.float32
    )
    return (new_max, row_total, weighted)


def local(
    residual,
    queries,
    latent,
    rope_key,
    doc_ids,
    latent_to_key,
    latent_to_value,
    out_proj,
    mix_gain,
    moe_gain,
    expert_ids,
    route_weight,
    gate_weight,
    up_weight,
    down_weight,
):
    local_rows = queries.shape[0]
    local_heads = queries.shape[1] // (UNROTATED_DIM + ROPE)
    query_pos = lax.axis_index("sp") * local_rows + jnp.arange(local_rows, dtype=jnp.int32)
    shaped = queries.reshape(local_rows, local_heads, UNROTATED_DIM + ROPE)
    query_nope = shaped[..., :UNROTATED_DIM]
    query_rot = rotate(shaped[..., UNROTATED_DIM:], query_pos)
    key_rot = rotate(rope_key, query_pos)
    initial = (
        jnp.full((local_rows, local_heads), -1e30, jnp.float32),
        jnp.zeros((local_rows, local_heads), jnp.float32),
        jnp.zeros((local_rows, local_heads, VALUE_ENTRIES), jnp.float32),
    )
    pieces = (
        lax.all_gather(latent, "sp", axis=0, tiled=True),
        lax.all_gather(key_rot, "sp", axis=0, tiled=True),
        lax.all_gather(doc_ids, "sp", axis=0, tiled=True),
    )
    row_count = pieces[0].shape[0]
    block_rows = math.gcd(row_count, 512)

    def one_block(number, current):
        first_row = number * block_rows
        sliced = [lax.dynamic_slice_in_dim(member, first_row, block_rows, 0) for member in pieces]
        key_pos = first_row + jnp.arange(block_rows, dtype=jnp.int32)
        active = (first_row <= query_pos[-1]) & (sliced[-1][-1] >= doc_ids[0])

        def compute(carried):
            key_nope = jnp.dot(sliced[0], latent_to_key, preferred_element_type=jnp.float32).astype(
                jnp.bfloat16
            )
            value_rows = jnp.dot(
                sliced[0], latent_to_value, preferred_element_type=jnp.float32
            ).astype(jnp.bfloat16)
            key_part = sliced[1]
            return attend_keys(
                carried,
                query_nope,
                query_rot,
                query_pos,
                doc_ids,
                key_nope.reshape(block_rows, local_heads, UNROTATED_DIM),
                key_part,
                value_rows.reshape(block_rows, local_heads, VALUE_ENTRIES),
                key_pos,
                sliced[-1],
            )

        return lax.cond(active, compute, lambda carried: carried, current)

    running = lax.fori_loop(0, row_count // block_rows, one_block, initial)
    attended = (running[2] / running[1][..., None]).astype(jnp.bfloat16)
    attended = attended.reshape(local_rows, local_heads * VALUE_ENTRIES)
    gathered = lax.all_to_all(attended, "tp", split_axis=0, concat_axis=1, tiled=True)
    mix = jnp.dot(gathered, out_proj, preferred_element_type=jnp.float32)
    branch = rms_scale(mix, mix_gain)
    middle = lax.optimization_barrier((residual.astype(jnp.float32) + branch).astype(jnp.bfloat16))
    normed = rms_scale(middle.astype(jnp.float32), moe_gain).astype(jnp.bfloat16)
    row_count = normed.shape[0]
    top_count = expert_ids.shape[1]
    expert_count = lax.axis_size("sp")
    capacity = row_count // (expert_count // GROUPS)
    flat_ids = expert_ids.reshape(-1)
    onehot = (flat_ids[:, None] == jnp.arange(expert_count, dtype=jnp.int32)[None, :]).astype(
        jnp.int32
    )
    earlier = jnp.cumsum(onehot, axis=0) - onehot
    slot_rank = jnp.sum(earlier * onehot, axis=1)
    slot_ids = (flat_ids * capacity + slot_rank).reshape(row_count, top_count)
    chooser = jnp.any(
        jnp.arange(expert_count * capacity, dtype=jnp.int32)[:, None, None] == slot_ids[None],
        axis=2,
    ).astype(jnp.bfloat16)
    buffer = jnp.dot(chooser, normed, preferred_element_type=jnp.float32).astype(jnp.bfloat16)
    buffer = buffer.reshape(expert_count, capacity, D)
    arrived = lax.all_to_all(buffer, "sp", split_axis=0, concat_axis=0, tiled=True)
    model_width = arrived.shape[2]
    both_halves = collect(arrived, "tp", 0)
    flat_rows = both_halves.reshape(-1, model_width)
    gate_out = jnp.dot(flat_rows, gate_weight[0], preferred_element_type=jnp.float32)
    upward = jnp.dot(flat_rows, up_weight[0], preferred_element_type=jnp.float32)
    hidden = (jax.nn.silu(gate_out) * upward).astype(jnp.bfloat16)
    partial_value = jnp.dot(hidden, down_weight[0], preferred_element_type=jnp.float32).reshape(
        both_halves.shape
    )
    summed = sum_at_owner(partial_value.astype(jnp.bfloat16), "tp", 0).astype(jnp.bfloat16)
    returned = lax.all_to_all(summed, "sp", split_axis=0, concat_axis=0, tiled=True)
    picked = returned.reshape(-1, D)[slot_ids.reshape(-1)].astype(jnp.float32)
    expert_mix = jnp.sum(
        (picked * route_weight.reshape(-1)[:, None]).reshape(row_count, top_count, D), axis=1
    )
    return (middle.astype(jnp.float32) + expert_mix).astype(jnp.bfloat16)


def solution(mesh):
    in_specs = (
        P(("sp", "tp"), None),
        P("sp", "tp"),
        P("sp", None),
        P("sp", None),
        P("sp"),
        P(None, "tp"),
        P(None, "tp"),
        P(),
        P(),
        P(),
        P(("sp", "tp"), None),
        P(("sp", "tp"), None),
        P("sp", None, "tp"),
        P("sp", None, "tp"),
        P("sp", "tp", None),
    )
    out_specs = P(("sp", "tp"), None)
    return jax.shard_map(local, mesh=mesh, in_specs=in_specs, out_specs=out_specs, check_vma=False)
```

profile of v0, /device:TPU:0, one launch (start us, length us, event | category | flops | bytes accessed | tf_op | source)
XLA Modules:
  0.0 649.7 jit_solution(9027320513454528965)
XLA Ops:
  10.0 1.6 slice.54
  13.5 186.6 %all-gather = s32[64,1,256]{2,1,0:T(1,128)} all-gather(s32[1,1,256]{2,1,0:T(1,128)} %bitcast.92), channel_id=1, replica_groups=mesh['sp'=64,'tp'=2] {'sp'}, dimensions={0}, use_global_device_ids=true | all-gather | bytes 66560 | tf_op jit(solution)/shard_map/all_gather | solution.py:129
  202.9 216.7 %while.17 = (s32[]{:T(128)}, f32[256,6]{0,1:T(8,128)S(1)}, f32[256,6]{0,1:T(8,128)S(1)}, f32[256,6,64]{0,2,1:T(8,128)S(1)}, s32[256]{0:T(256)}, /*index=5*/s32[1...) while((s32[]{:T(128)}, f32[256,6]{0,1:T(8,128)S(1)}, ...), condition=%wide.region_5.6_spmd, body=%wide.region_0.5_spmd.sunk | while | flops 461835776 | bytes 21579896 | solution.py:163
  205.0 1.2 slice.72
  207.4 1.3 slice.70
  209.5 7.0 %conditional.2 = ((f32[256,6]{0,1:T(8,128)S(1)}, f32[256,6]{0,1:T(8,128)S(1)}, f32[256,6,64]{0,2,1:T(8,128)S(1)})) conditional(s32[]{:T(128)} %convert_element_type.177, (f32[256,6]{0,1:T(8,128)S(1)}, f32[256,6]{0,1:T(8,128)S(1)}, f32[256,6,64]{0,2,1:T(8,128)S(1)}) %tuple.50, (s32[]{:T(128)}, s32[512]{0:T(512)}, s32[256]{0:T(256)}, s32[512]{0:T(512)}, ...), branch_computations={%region_1.0_spmd, %region_2.4_spmd} | conditional | flops 461835776 | bytes 21565132 | solution.py:161
  209.5 1.3 convolution_convert_fusion.1
  210.9 1.5 fusion.16
  214.5 1.2 convolution_convert_fusion
  218.5 1.2 slice.72
  221.0 1.3 slice.70
  225.1 1.2 slice.72
  227.5 1.3 slice.70
  234.1 1.3 slice.70
  238.2 1.2 slice.72
  240.6 1.3 slice.70
  244.7 1.2 slice.72
  247.2 1.3 slice.70
  251.3 1.2 slice.72
  253.7 1.3 slice.70
  257.8 1.2 slice.72
  260.3 1.3 slice.70
  264.4 1.2 slice.72
  266.8 1.3 slice.70
  270.9 1.2 slice.72
  273.4 1.3 slice.70
  277.5 1.2 slice.72
  279.9 1.3 slice.70
  284.0 1.2 slice.72
  286.5 1.3 slice.70
  293.1 1.3 slice.70
  299.6 1.3 slice.70
  306.2 1.3 slice.70
  312.7 1.3 slice.70
  319.3 1.3 slice.70
  325.9 1.3 slice.70
  332.4 1.3 slice.70
  339.0 1.3 slice.70
  345.5 1.3 slice.70
  352.1 1.3 slice.70
  358.6 1.3 slice.70
  365.2 1.3 slice.70
  371.7 1.3 slice.70
  378.3 1.3 slice.70
  384.8 1.3 slice.70
  391.4 1.3 slice.70
  398.0 1.3 slice.70
  404.5 1.3 slice.70
  411.1 1.3 slice.70
  417.6 1.3 slice.70
  421.4 4.0 all_to_all.39
  428.0 137.1 %all_to_all.40 = bf16[64,8,2048]{2,1,0:T(8,128)(2,1)S(1)} all-to-all(bf16[64,8,2048]{2,1,0:T(8,128)(2,1)S(1)} %fusion.23), channel_id=1, replica_groups=mesh['sp'=64,'tp'=2] {'sp'}, dimensions={0} | all-to-all | bytes 4194304 | tf_op jit(solution)/shard_map/all_to_all | solution.py:188
  565.6 7.2 %all_to_all.41 = bf16[2,64,8,2048]{3,2,1,0:T(8,128)(2,1)S(1)} all-to-all(bf16[2,64,8,2048]{3,2,1,0:T(8,128)(2,1)S(1)} %broadcast_in_dim.63), channel_id=1, replica_groups=mesh['sp'=64,'tp'=2] {'tp'}, dimensions={0} | all-to-all | bytes 8388608 | tf_op jit(solution)/shard_map/all_to_all | solution.py:24
  572.8 2.3 fusion.25
  575.2 2.6 fusion.31
  577.8 2.4 convolution_convert_fusion.2
  580.8 8.2 %all_to_all.42 = bf16[2,64,8,2048]{3,1,2,0:T(8,128)(2,1)} all-to-all(bf16[2,64,8,2048]{3,1,2,0:T(8,128)(2,1)S(1)} %copy.65), channel_id=1, replica_groups=mesh['sp'=64,'tp'=2] {'tp'}, dimensions={0} | all-to-all | bytes 8388608 | tf_op jit(solution)/shard_map/all_to_all | solution.py:38
  589.0 3.5 reduce_sum.67
  592.5 2.5 copy.67
  595.0 6.1 all-to-all-start.4
  601.3 29.9 %all-to-all-done.4 = bf16[64,8,2048]{2,1,0:T(8,128)(2,1)S(1)} async-done(((bf16[64,8,2048]{2,1,0:T(8,128)(2,1)}), bf16[64,8,2048]{2,1,0:T(8,128)(2,1)S(1)}, u32[]{:S(2)}, u32[]{:S(2)}) %all-to-all-start.4) | async-done | bytes 2097184 | tf_op jit(solution)/shard_map/all_to_all | solution.py:199
  631.2 2.3 gather_fusion
  633.5 3.5 reshape.226
  637.1 4.9 multiply_reduce_fusion
  (307 shorter events, 107.1 us)
Async XLA Ops:
  6.5 418.9 %copy-start = (bf16[768,2048]{1,0:T(8,128)(2,1)S(1)}, bf16[768,2048]{1,0:T(8,128)(2,1)}, u32[]{:S(2)}) copy-start(bf16[768,2048]{1,0:T(8,128)(2,1)} %param.26) | copy-start | bytes 9437188
  6.5 196.3 %all-gather.6.cloned.1.call-start = ((), (), s32[]{:S(2)}) async-start(), calls=%async_computation.6 | async-start | bytes 1064960 | tf_op jit(solution)/shard_map/all_gather | solution.py:128
  8.2 194.6 %all-gather.4.cloned.1.call-start = ((), (), s32[]{:S(2)}) async-start(), calls=%async_computation.5 | async-start | bytes 8519680 | tf_op jit(solution)/shard_map/all_gather | solution.py:127
  12.6 190.2 %copy-start.14 = (s32[256]{0:T(256)}, s32[256]{0:T(256)S(1)}, u32[]{:S(2)}) copy-start(s32[256]{0:T(256)S(1)} %fusion.49) | copy-start | bytes 3076
  203.7 0.6 copy-start.9
  209.5 2.9 copy-start.11
  209.5 2.9 copy-start.10
  209.5 2.9 copy-start.12
  209.5 2.9 copy-start.13
  209.5 3.1 copy-start.4
  213.5 0.9 copy-start.5
  217.2 0.6 copy-start.9
  223.8 0.6 copy-start.9
  230.4 0.6 copy-start.9
  236.9 0.6 copy-start.9
  243.5 0.6 copy-start.9
  250.0 0.6 copy-start.9
  256.6 0.6 copy-start.9
  263.1 0.6 copy-start.9
  269.7 0.6 copy-start.9
  276.2 0.6 copy-start.9
  282.8 0.6 copy-start.9
  289.3 0.6 copy-start.9
  295.9 0.6 copy-start.9
  302.5 0.6 copy-start.9
  309.0 0.6 copy-start.9
  315.6 0.6 copy-start.9
  322.1 0.6 copy-start.9
  328.7 0.6 copy-start.9
  335.3 0.6 copy-start.9
  341.8 0.6 copy-start.9
  348.4 0.6 copy-start.9
  354.9 0.6 copy-start.9
  361.5 0.6 copy-start.9
  368.0 0.6 copy-start.9
  374.6 0.6 copy-start.9
  381.1 0.6 copy-start.9
  387.7 0.6 copy-start.9
  394.2 0.6 copy-start.9
  400.8 0.6 copy-start.9
  407.3 0.6 copy-start.9
  413.9 0.6 copy-start.9
  419.7 6.5 copy-start.16
  421.4 4.8 copy-start.6
  425.5 1.7 copy-start.7
  425.5 1.7 copy-start.17
  426.4 0.8 copy-start.2
  565.6 7.2 %copy-start.19 = (bf16[1,2048,512]{2,1,0:T(8,128)(2,1)S(1)}, bf16[1,2048,512]{2,1,0:T(8,128)(2,1)}, u32[]{:S(2)}) copy-start(bf16[1,2048,512]{2,1,0:T(8,128)(2,1)} %param.32) | copy-start | bytes 6291460
  572.8 2.3 copy-start.20
  575.2 2.7 copy-start.21
  595.0 6.1 copy-start.8
  595.0 6.2 copy-start.18
  595.0 6.4 copy-start.15
  595.0 36.2 %all-to-all-start.4 = ((bf16[64,8,2048]{2,1,0:T(8,128)(2,1)}), bf16[64,8,2048]{2,1,0:T(8,128)(2,1)S(1)}, u32[]{:S(2)}, u32[]{:S(2)}) async-start(bf16[64,8,2048]{2,1,0:T(8,128)(2,1)} %copy.67), calls=%async_computation.4 | async-start | bytes 4194304 | tf_op jit(solution)/shard_map/all_to_all | solution.py:199
  633.5 9.3 %copy-start.1 = (bf16[768,2048]{1,0:T(8,128)(2,1)S(1)}, bf16[768,2048]{1,0:T(8,128)(2,1)}, u32[]{:S(2)}) copy-start(bf16[768,2048]{1,0:T(8,128)(2,1)} %param.26) | copy-start | bytes 9437188
  637.1 4.9 copy-start.3
Sparse Core Ops, SparseCore 0:
  10.0 66.1 all-gather.5
  79.0 76.5 all-gather.3
where the time goes:
time: 655 us; the launch traced here: 650 us
  blocking collectives  343 us (52%)
  local copies, waits for them, and re-layouts  160 us (24%)
  loops' own time  64.4 us (10%)
  waiting for transfers between devices  30.6 us (5%)
  other arithmetic  17 us (3%)
  matrix products  14.5 us (2%)
  between operations  13.7 us (2%)
    all_gather x1, blocking collectives, local(): lax.all_gather(doc_ids, 'sp', axis=0, tiled=True)  187 us
    all_to_all x1, blocking collectives, local(): lax.all_to_all(buffer, 'sp', split_axis=0, concat_axis=0, tiled=True)  137 us
    slice x96, local copies, waits for them, and re-layouts, one_block(): active = (first_row <= query_pos[-1]) & (sliced[-1][-1] >= doc_ids[0])  102 us
    another operation x1, loops' own time, local(): running = lax.fori_loop(0, row_count // block_rows, one_block, initial)  63.9 us
    all_to_all x1, waiting for transfers between devices, local(): lax.all_to_all(summed, 'sp', split_axis=0, concat_axis=0, tiled=True)  29.9 us
    dynamic_slice x32, local copies, waits for them, and re-layouts, one_block(): lax.dynamic_slice_in_dim(member, first_row, block_rows, 0)  24.2 us
    iota x32, local copies, waits for them, and re-layouts, one_block(): key_pos = first_row + jnp.arange(block_rows, dtype=jnp.int32)  19.1 us
  transfers between devices with their start and end apart: 3, of which 1 were waited for; matrix products, arithmetic and copies ran while one was open for 1% of the time, Pallas kernels for 0%

commit v1 on v0

--- a/solution.py
+++ b/solution.py
@@ -11,6 +11,11 @@
 GROUPS = 4
 rope_base = 10000.0
 epsilon = 1e-06
+
+
+def gather_by_exchange(array, axis, dim):
+    copies = jnp.concatenate([array] * lax.axis_size(axis), axis=dim)
+    return lax.all_to_all(copies, axis, dim, dim, tiled=True)
 
 
 def in_order(pieces, dim):
@@ -126,7 +131,7 @@
     pieces = (
         lax.all_gather(latent, "sp", axis=0, tiled=True),
         lax.all_gather(key_rot, "sp", axis=0, tiled=True),
-        lax.all_gather(doc_ids, "sp", axis=0, tiled=True),
+        gather_by_exchange(doc_ids, "sp", 0),
     )
     row_count = pieces[0].shape[0]
     block_rows = math.gcd(row_count, 512)

time: 655 us -> 607 us (0.927)
  blocking collectives: 343 us -> 163 us
  waiting for transfers between devices: 30.6 us -> 157 us
  starting transfers between devices: 6.11 us -> 17.6 us
    all_gather x1 -> x0, blocking collectives: 187 us -> none  [local(): lax.all_gather(doc_ids, 'sp', axis=0, tiled=True)]
    all_gather x1, waiting for transfers between devices: 0.01 us -> 79.3 us  [local(): lax.all_gather(latent, 'sp', axis=0, tiled=True)]
    all_gather x1, waiting for transfers between devices: 0.01 us -> 44.8 us  [local(): lax.all_gather(key_rot, 'sp', axis=0, tiled=True)]
    all_to_all x0 -> x1, starting transfers between devices: none -> 11.5 us  [gather_by_exchange(): return lax.all_to_all(copies, axis, dim, dim, tiled=True)]
  transfers between devices with their start and end apart: 3 -> 4, of which waited for: 1 -> 4; matrix products, arithmetic and copies ran while one was open for 1% -> 1% of each run, Pallas kernels for 0% -> 0%
where the time goes in v1:
time: 607 us; the launch traced here: 601 us
  blocking collectives  163 us (27%)
  local copies, waits for them, and re-layouts  158 us (26%)
  waiting for transfers between devices  157 us (26%)
  loops' own time  60.8 us (10%)
  starting transfers between devices  17.6 us (3%)
  other arithmetic  16.9 us (3%)
  matrix products  14.5 us (2%)
  between operations  13.7 us (2%)
    all_to_all x1, blocking collectives, local(): lax.all_to_all(buffer, 'sp', split_axis=0, concat_axis=0, tiled=True)  143 us
    slice x96, local copies, waits for them, and re-layouts, one_block(): active = (first_row <= query_pos[-1]) & (sliced[-1][-1] >= doc_ids[0])  99 us
    all_gather x1, waiting for transfers between devices, local(): lax.all_gather(latent, 'sp', axis=0, tiled=True)  79.3 us
    another operation x1, loops' own time, local(): running = lax.fori_loop(0, row_count // block_rows, one_block, initial)  60.3 us
    all_gather x1, waiting for transfers between devices, local(): lax.all_gather(key_rot, 'sp', axis=0, tiled=True)  44.8 us
    all_to_all x1, waiting for transfers between devices, local(): lax.all_to_all(summed, 'sp', split_axis=0, concat_axis=0, tiled=True)  29.9 us
    dynamic_slice x32, local copies, waits for them, and re-layouts, one_block(): lax.dynamic_slice_in_dim(member, first_row, block_rows, 0)  24.2 us
    iota x32, local copies, waits for them, and re-layouts, one_block(): key_pos = first_row + jnp.arange(block_rows, dtype=jnp.int32)  18.9 us
  transfers between devices with their start and end apart: 4, of which 4 were waited for; matrix products, arithmetic and copies ran while one was open for 1% of the time, Pallas kernels for 0%

profile of v1, /device:TPU:0, one launch (start us, length us, event | category | flops | bytes accessed | tf_op | source)
XLA Modules:
  0.0 601.5 jit_solution(3958371682289738184)
XLA Ops:
  9.0 1.3 concatenate.12
  10.3 11.5 %all-to-all-start = ((s32[64,256,1]{1,2,0:T(1,128)}), s32[64,256,1]{1,2,0:T(1,128)S(1)}, u32[]{:S(2)}, u32[]{:S(2)}) async-start(s32[64,256,1]{1,2,0:T(1,128)} %concatenate.12), calls=%async_computation | async-start | bytes 131072 | tf_op jit(solution)/shard_map/all_to_all | solution.py:18
  22.9 1.6 slice.54
  29.1 2.3 all-to-all-done
  31.4 44.8 %all-gather.5.cloned.1.call-done = bf16[16384,32]{0,1:T(8,128)(2,1)} async-done(((bf16[256,32]{0,1:T(8,128)(2,1)}), bf16[16384,32]{0,1:T(8,128)(2,1)}) %all-gather.5.cloned.1.call-update) | async-done | bytes 1048592 | tf_op jit(solution)/shard_map/all_gather | solution.py:133
  76.2 79.3 %all-gather.3.cloned.1.call-done = bf16[16384,256]{1,0:T(8,128)(2,1)} async-done(((bf16[256,256]{1,0:T(8,128)(2,1)}), bf16[16384,256]{1,0:T(8,128)(2,1)}) %all-gather.3.cloned.1.call-update) | async-done | bytes 8388624 | tf_op jit(solution)/shard_map/all_gather | solution.py:132
  155.6 209.8 %while.17 = (s32[]{:T(128)}, f32[256,6]{0,1:T(8,128)S(1)}, f32[256,6]{0,1:T(8,128)S(1)}, f32[256,6,64]{0,2,1:T(8,128)S(1)}, s32[256]{0:T(256)}, /*index=5*/s32[1...) while((s32[]{:T(128)}, f32[256,6]{0,1:T(8,128)S(1)}, ...), condition=%wide.region_5.6_spmd, body=%wide.region_0.5_spmd.sunk | while | flops 461835776 | bytes 21579896 | solution.py:168
  160.0 1.3 slice.70
  161.9 7.0 %conditional.2 = ((f32[256,6]{0,1:T(8,128)S(1)}, f32[256,6]{0,1:T(8,128)S(1)}, f32[256,6,64]{0,2,1:T(8,128)S(1)})) conditional(s32[]{:T(128)} %convert_element_type.177, (f32[256,6]{0,1:T(8,128)S(1)}, f32[256,6]{0,1:T(8,128)S(1)}, f32[256,6,64]{0,2,1:T(8,128)S(1)}) %tuple.50, (s32[]{:T(128)}, s32[512]{0:T(512)}, s32[256]{0:T(256)}, s32[512]{0:T(512)}, ...), branch_computations={%region_1.0_spmd, %region_2.4_spmd} | conditional | flops 461835776 | bytes 21565132 | solution.py:166
  162.0 1.3 convolution_convert_fusion.1
  163.3 1.5 fusion.16
  166.9 1.2 convolution_convert_fusion
  170.9 1.2 slice.72
  173.3 1.3 slice.70
  177.3 1.2 slice.72
  179.7 1.3 slice.70
  186.0 1.3 slice.70
  192.3 1.3 slice.70
  196.3 1.2 slice.72
  198.7 1.3 slice.70
  205.0 1.3 slice.70
  211.3 1.3 slice.70
  217.7 1.3 slice.70
  224.0 1.3 slice.70
  230.4 1.3 slice.70
  234.3 1.2 slice.72
  236.7 1.3 slice.70
  243.1 1.3 slice.70
  249.4 1.3 slice.70
  253.3 1.2 slice.72
  255.7 1.3 slice.70
  259.7 1.2 slice.72
  262.1 1.3 slice.70
  268.4 1.3 slice.70
  272.3 1.2 slice.72
  274.7 1.3 slice.70
  281.1 1.3 slice.70
  287.4 1.3 slice.70
  293.7 1.3 slice.70
  300.1 1.3 slice.70
  306.4 1.3 slice.70
  312.8 1.3 slice.70
  319.1 1.3 slice.70
  325.4 1.3 slice.70
  331.8 1.3 slice.70
  338.1 1.3 slice.70
  344.4 1.3 slice.70
  350.8 1.3 slice.70
  357.1 1.3 slice.70
  363.5 1.3 slice.70
  367.1 4.0 all_to_all.48
  373.7 143.2 %all_to_all.49 = bf16[64,8,2048]{2,1,0:T(8,128)(2,1)S(1)} all-to-all(bf16[64,8,2048]{2,1,0:T(8,128)(2,1)S(1)} %fusion.23), channel_id=1, replica_groups=mesh['sp'=64,'tp'=2] {'sp'}, dimensions={0} | all-to-all | bytes 4194304 | tf_op jit(solution)/shard_map/all_to_all | solution.py:193
  517.4 7.2 %all_to_all.50 = bf16[2,64,8,2048]{3,2,1,0:T(8,128)(2,1)S(1)} all-to-all(bf16[2,64,8,2048]{3,2,1,0:T(8,128)(2,1)S(1)} %broadcast_in_dim.63), channel_id=1, replica_groups=mesh['sp'=64,'tp'=2] {'tp'}, dimensions={0} | all-to-all | bytes 8388608 | tf_op jit(solution)/shard_map/all_to_all | solution.py:29
  524.7 2.3 fusion.25
  527.0 2.6 fusion.31
  529.7 2.4 convolution_convert_fusion.2
  532.6 8.2 %all_to_all.51 = bf16[2,64,8,2048]{3,1,2,0:T(8,128)(2,1)} all-to-all(bf16[2,64,8,2048]{3,1,2,0:T(8,128)(2,1)S(1)} %copy.65), channel_id=1, replica_groups=mesh['sp'=64,'tp'=2] {'tp'}, dimensions={0} | all-to-all | bytes 8388608 | tf_op jit(solution)/shard_map/all_to_all | solution.py:43
  540.8 3.5 reduce_sum.67
  544.3 2.5 copy.67
  546.8 6.1 %all-to-all-start.5 = ((bf16[64,8,2048]{2,1,0:T(8,128)(2,1)}), bf16[64,8,2048]{2,1,0:T(8,128)(2,1)S(1)}, u32[]{:S(2)}, u32[]{:S(2)}) async-start(bf16[64,8,2048]{2,1,0:T(8,128)(2,1)} %copy.67), calls=%async_computation.5 | async-start | bytes 4194304 | tf_op jit(solution)/shard_map/all_to_all | solution.py:204
  553.1 29.9 %all-to-all-done.5 = bf16[64,8,2048]{2,1,0:T(8,128)(2,1)S(1)} async-done(((bf16[64,8,2048]{2,1,0:T(8,128)(2,1)}), bf16[64,8,2048]{2,1,0:T(8,128)(2,1)S(1)}, u32[]{:S(2)}, u32[]{:S(2)}) %all-to-all-start.5) | async-done | bytes 2097184 | tf_op jit(solution)/shard_map/all_to_all | solution.py:204
  583.0 2.3 gather_fusion
  585.3 3.5 reshape.294
  588.9 4.9 multiply_reduce_fusion
  (311 shorter events, 111.3 us)
Async XLA Ops:
  6.5 364.6 %copy-start = (bf16[768,2048]{1,0:T(8,128)(2,1)S(1)}, bf16[768,2048]{1,0:T(8,128)(2,1)}, u32[]{:S(2)}) copy-start(bf16[768,2048]{1,0:T(8,128)(2,1)} %param.26) | copy-start | bytes 9437188
  6.5 69.6 %all-gather.5.cloned.1.call-start = ((), (), s32[]{:S(2)}) async-start(), calls=%async_computation.7 | async-start | bytes 1064960 | tf_op jit(solution)/shard_map/all_gather | solution.py:133
  8.2 147.3 %all-gather.3.cloned.1.call-start = ((), (), s32[]{:S(2)}) async-start(), calls=%async_computation.6 | async-start | bytes 8519680 | tf_op jit(solution)/shard_map/all_gather | solution.py:132
  10.3 21.1 %all-to-all-start = ((s32[64,256,1]{1,2,0:T(1,128)}), s32[64,256,1]{1,2,0:T(1,128)S(1)}, u32[]{:S(2)}, u32[]{:S(2)}) async-start(s32[64,256,1]{1,2,0:T(1,128)} %concatenate.12), calls=%async_computation | async-start | bytes 131072 | tf_op jit(solution)/shard_map/all_to_all | solution.py:18
  25.5 130.0 %copy-start.15 = (s32[256]{0:T(256)}, s32[256]{0:T(256)S(1)}, u32[]{:S(2)}) copy-start(s32[256]{0:T(256)S(1)} %fusion.49) | copy-start | bytes 3076
  31.4 124.1 %copy-start.12 = (s32[64,256,1]{1,2,0:T(1,128)}, s32[64,256,1]{1,2,0:T(1,128)S(1)}, u32[]{:S(2)}) copy-start(s32[64,256,1]{1,2,0:T(1,128)S(1)} %all-to-all-done) | copy-start | bytes 196612
  156.3 0.6 copy-start.9
  161.9 2.9 copy-start.11
  161.9 2.9 copy-start.10
  161.9 2.9 copy-start.13
  161.9 2.9 copy-start.14
  161.9 3.1 copy-start.4
  166.0 0.9 copy-start.5
  169.7 0.6 copy-start.9
  176.0 0.6 copy-start.9
  182.4 0.6 copy-start.9
  188.7 0.6 copy-start.9
  195.0 0.6 copy-start.9
  201.4 0.6 copy-start.9
  207.7 0.6 copy-start.9
  214.0 0.6 copy-start.9
  220.4 0.6 copy-start.9
  226.7 0.6 copy-start.9
  233.1 0.6 copy-start.9
  239.4 0.6 copy-start.9
  245.8 0.6 copy-start.9
  252.1 0.6 copy-start.9
  258.4 0.6 copy-start.9
  264.8 0.6 copy-start.9
  271.1 0.6 copy-start.9
  277.4 0.6 copy-start.9
  283.8 0.6 copy-start.9
  290.1 0.6 copy-start.9
  296.4 0.6 copy-start.9
  302.8 0.6 copy-start.9
  309.1 0.6 copy-start.9
  315.5 0.6 copy-start.9
  321.8 0.6 copy-start.9
  328.1 0.6 copy-start.9
  334.5 0.6 copy-start.9
  340.8 0.6 copy-start.9
  347.1 0.6 copy-start.9
  353.5 0.6 copy-start.9
  359.8 0.6 copy-start.9
  365.4 6.5 %copy-start.17 = (f32[2048]{0:T(1024)S(1)}, f32[2048]{0:T(1024)}, u32[]{:S(2)}) copy-start(f32[2048]{0:T(1024)} %param.27) | copy-start | bytes 24580
  367.1 4.8 copy-start.6
  371.2 1.7 copy-start.7
  371.2 1.7 copy-start.18
  372.1 0.8 copy-start.2
  517.4 7.2 %copy-start.20 = (bf16[1,2048,512]{2,1,0:T(8,128)(2,1)S(1)}, bf16[1,2048,512]{2,1,0:T(8,128)(2,1)}, u32[]{:S(2)}) copy-start(bf16[1,2048,512]{2,1,0:T(8,128)(2,1)} %param.32) | copy-start | bytes 6291460
  524.7 2.3 copy-start.21
  527.0 2.7 copy-start.22
  546.7 6.1 %copy-start.8 = (s32[128,2]{1,0:T(8,128)S(1)}, s32[128,2]{1,0:T(8,128)}, u32[]{:S(2)}) copy-start(s32[128,2]{1,0:T(8,128)} %get-tuple-element.385) | copy-start | bytes 3076
  546.8 6.2 %copy-start.19 = (f32[128,2]{0,1:T(2,128)S(1)}, f32[128,2]{0,1:T(2,128)}, u32[]{:S(2)}) copy-start(f32[128,2]{0,1:T(2,128)} %param.30) | copy-start | bytes 3076
  546.8 6.4 %copy-start.16 = (s32[256]{0:T(256)S(1)}, s32[256]{0:T(256)}, u32[]{:S(2)}) copy-start(s32[256]{0:T(256)} %copy-done.15) | copy-start | bytes 3076
  546.8 36.2 %all-to-all-start.5 = ((bf16[64,8,2048]{2,1,0:T(8,128)(2,1)}), bf16[64,8,2048]{2,1,0:T(8,128)(2,1)S(1)}, u32[]{:S(2)}, u32[]{:S(2)}) async-start(bf16[64,8,2048]{2,1,0:T(8,128)(2,1)} %copy.67), calls=%async_computation.5 | async-start | bytes 4194304 | tf_op jit(solution)/shard_map/all_to_all | solution.py:204
  585.3 9.3 %copy-start.1 = (bf16[768,2048]{1,0:T(8,128)(2,1)S(1)}, bf16[768,2048]{1,0:T(8,128)(2,1)}, u32[]{:S(2)}) copy-start(bf16[768,2048]{1,0:T(8,128)(2,1)} %param.26) | copy-start | bytes 9437188
  588.9 4.9 copy-start.3
Sparse Core Ops, SparseCore 0:
  10.0 66.1 all-gather.4
  79.0 76.4 all-gather.2
